TPU v7x, 512 devices: a whole 4x4x16 slice. The times are simulated.
512 devices in a mesh: sp: 32 (over z, core), tp: 16 (over y, x).
Axes of the slice: x: 4, y: 4, z: 16, core: 2. Of those that a mesh axis runs over, the one named last changes fastest.
Arguments:
- queries: bfloat16 [16384, 1024], P('sp', 'tp'), may hold values from -20 to 20
- key_vectors: bfloat16 [16384, 1024], P('sp', 'tp'), may hold values from -20 to 20
- value_vectors: bfloat16 [16384, 1024], P('sp', 'tp'), may hold values from -6 to 6
- log_gate_sums: float32 [16384, 16], P('sp', 'tp'), may hold values from -2343 to 0, as said below
- residual: bfloat16 [16384, 2048], P('sp', 'tp'), may hold values from -24 to 24
- out_weight: bfloat16 [1024, 2048], P(None, 'tp'), may hold values from -0.75 to 0.75
- norm_gain: bfloat16 [2048], replicated, may hold values from 0.099609375 to 1.8984375
- routes: int32 [16384, 2], P('sp'), may hold values from 0 to 127, all different within a row; in each aligned block of 512 rows (0 to 511, 512 to 1023, ...) at most 10 rows name the same one
- route_weight: float32 [16384, 2], P('sp'), may hold values from 0.5 to 1.5
- expert_gate: bfloat16 [128, 2048, 512], P('sp', None, 'tp'), may hold values from -0.125 to 0.125
- expert_up: bfloat16 [128, 2048, 512], P('sp', None, 'tp'), may hold values from -0.125 to 0.125
- expert_down: bfloat16 [128, 512, 2048], P('sp', None, 'tp'), may hold values from -0.25 to 0.25
- shared_gate: bfloat16 [2048, 512], P(None, 'tp'), may hold values from -0.125 to 0.125
- shared_up: bfloat16 [2048, 512], P(None, 'tp'), may hold values from -0.125 to 0.125
- shared_down: bfloat16 [512, 2048], P(None, 'tp'), may hold values from -0.25 to 0.25
Outputs:
- layer_out: bfloat16 [16384, 2048], P('sp', 'tp')
Inputs may be any that keep to these rules, and one draw needn't show every extreme that they name: `log_gate_sums`: for each head the values do not rise along the positions. `routes`: each row names 2 different experts; among the rows of one index of sp no expert is named by more than 10 rows, a bound that some block reaches.
All inputs are finite; a program needn't handle non-finite values.
Results may differ from a plain program's by a relative error of at most 0.014.
Values may be sent and summed in bfloat16 or wider, within the bound.
No kernel may reach another device: no remote copies, remote signals or barrier semaphores. Data moves between devices by JAX's collectives and lax.ppermute only.
A program may use at most 64 MiB of HBM per device.

v0:
```python
import math
import jax
import jax.numpy as jnp
from jax import lax
from jax.sharding import PartitionSpec as P

HDIM = 64
EPSILON = 1e-06


def in_one_piece(arrays, axis, dim, along):
    both = jnp.concatenate(arrays, axis=along)
    filled, at, done = (lax.all_gather(both, axis, axis=dim, tiled=True), 0, [])
    for a in arrays:
        done.append(lax.slice_in_dim(filled, at, at + a.shape[along], axis=along))
        at += a.shape[along]
    return tuple(done)


def joined_along(tiles, dim):
    lengths = list(tiles.shape[1:])
    lengths[dim] *= tiles.shape[0]
    return jnp.moveaxis(tiles, 0, dim).reshape(lengths)


def sent_to_all(array, axis):
    copies = jnp.broadcast_to(array, (lax.axis_size(axis), *array.shape))
    return lax.all_to_all(copies, axis, split_axis=0, concat_axis=0, tiled=True)


def gather_directly(array, axis, dim):
    return joined_along(sent_to_all(array, axis), dim)


def over_copies(array, axis):
    everything = sent_to_all(array, axis)
    return jnp.sum(everything, axis=0)


def silu_gate(gate_part, up_part):
    return jax.nn.silu(gate_part) * up_part


def slot_targets(routes, experts_all, capacity):
    flat_routes = routes.reshape(-1)
    onehot = (flat_routes[:, None] == jnp.arange(experts_all, dtype=jnp.int32)[None, :]).astype(
        jnp.int32
    )
    before = jnp.cumsum(onehot, axis=0) - onehot
    return flat_routes * capacity + jnp.sum(before * onehot, axis=1)


def keep_state(fold_state):
    return fold_state


def shards(
    queries,
    key_vectors,
    value_vectors,
    log_gate_sums,
    residual,
    out_weight,
    norm_gain,
    routes,
    route_weight,
    expert_gate,
    expert_up,
    expert_down,
    shared_gate,
    shared_up,
    shared_down,
):
    tok_dev = queries.shape[0]
    head_dim = HDIM
    local_heads = log_gate_sums.shape[1]
    local_width = residual.shape[1]
    model_width = norm_gain.shape[0]
    score_scale = head_dim ** (-0.5)
    seq_first = lax.axis_index("sp") * tok_dev
    query_heads = queries.reshape(tok_dev, local_heads, head_dim)
    query_pos = seq_first + jnp.arange(tok_dev, dtype=jnp.int32)
    own_gates = log_gate_sums.T
    all_gates = lax.all_gather(log_gate_sums, "sp", axis=0, tiled=True)
    initial = (
        jnp.full((local_heads, tok_dev), -1e30, jnp.float32),
        jnp.zeros((local_heads, tok_dev), jnp.float32),
        jnp.zeros((local_heads, tok_dev, head_dim), jnp.float32),
    )
    key_heads = key_vectors.reshape(tok_dev, local_heads, head_dim)
    value_heads = value_vectors.reshape(tok_dev, local_heads, head_dim)
    key_part, value_part = in_one_piece((key_heads, value_heads), "sp", 0, 1)
    part_rows = key_part.shape[0]
    block_size = math.gcd(part_rows, 512)
    key_blocks = key_part.reshape(part_rows // block_size, block_size, local_heads, head_dim)
    value_blocks = value_part.reshape(part_rows // block_size, block_size, local_heads, head_dim)

    def one_block(fold_state, inputs):
        key_block, value_block, block_number = inputs
        block_first = block_number * block_size

        def compute(old_state):
            running_max, weight_total, summed = old_state
            gate_block = lax.dynamic_slice_in_dim(all_gates, block_first, block_size, 0).T
            scores = (
                jnp.einsum(
                    "qhd,khd->hqk", query_heads, key_block, preferred_element_type=jnp.float32
                )
                * score_scale
            )
            scores = scores + own_gates[:, :, None] - gate_block[:, None, :]
            key_pos = block_first + jnp.arange(block_size, dtype=jnp.int32)
            allowed = (key_pos[None, :] <= query_pos[:, None])[None]
            newmax = jnp.maximum(running_max, jnp.max(jnp.where(allowed, scores, -jnp.inf), axis=2))
            factor = jnp.exp(running_max - newmax)
            weight = jnp.where(allowed, jnp.exp(scores - newmax[:, :, None]), 0.0)
            weight_total = weight_total * factor + jnp.sum(weight, axis=2)
            summed = summed * factor[:, :, None] + jnp.einsum(
                "hqk,khd->hqd",
                weight.astype(jnp.bfloat16),
                value_block,
                preferred_element_type=jnp.float32,
            )
            return (newmax, weight_total, summed)

        useful = block_first <= seq_first + tok_dev - 1
        return (lax.cond(useful, compute, keep_state, fold_state), None)

    numbers = jnp.arange(part_rows // block_size, dtype=jnp.int32)
    result_state, _ = lax.scan(one_block, initial, (key_blocks, value_blocks, numbers))
    running_max, weight_total, summed = result_state
    attended = (summed / weight_total[:, :, None]).astype(jnp.bfloat16)
    attended = attended.transpose(1, 0, 2).reshape(tok_dev, local_heads * head_dim)
    weight_rows = out_weight
    projected = jnp.dot(
        gather_directly(attended, "tp", 1), weight_rows, preferred_element_type=jnp.float32
    )
    mid = (residual.astype(jnp.float32) + projected).astype(jnp.bfloat16)
    mid_wide = mid.astype(jnp.float32)
    feature_first = lax.axis_index("tp") * local_width
    squares = over_copies(jnp.sum(mid_wide * mid_wide, axis=1), "tp")
    inverse = lax.rsqrt(squares / model_width + EPSILON)
    own_gain = lax.dynamic_slice_in_dim(norm_gain, feature_first, local_width, 0).astype(
        jnp.float32
    )
    normed_own = (mid_wide * inverse[:, None] * own_gain[None, :]).astype(jnp.bfloat16)
    normed = gather_directly(normed_own, "tp", 1)
    shared_mid = silu_gate(
        jnp.dot(normed, shared_gate, preferred_element_type=jnp.float32),
        jnp.dot(normed, shared_up, preferred_element_type=jnp.float32),
    ).astype(jnp.bfloat16)
    weight_rows = shared_down
    shared_out = jnp.dot(
        lax.all_gather(shared_mid, "tp", axis=1, tiled=True),
        weight_rows,
        preferred_element_type=jnp.float32,
    )
    exp_dev = expert_gate.shape[0]
    sp_count = lax.axis_size("sp")
    experts_all = exp_dev * sp_count
    top_count = routes.shape[1]
    capacity = 5 * tok_dev * top_count // (4 * experts_all)
    targets = slot_targets(routes, experts_all, capacity)
    owners = (
        jnp.full((experts_all * capacity,), tok_dev, jnp.int32)
        .at[targets]
        .set(jnp.arange(tok_dev * top_count, dtype=jnp.int32) // top_count)
    )
    padded = jnp.concatenate(
        [normed_own, jnp.zeros((1, normed_own.shape[1]), jnp.bfloat16)], axis=0
    )
    outgoing = padded[owners].reshape(sp_count, exp_dev, capacity, normed_own.shape[1])
    rows_all = lax.all_gather(
        lax.all_to_all(outgoing, "sp", split_axis=0, concat_axis=0, tiled=True),
        "tp",
        axis=3,
        tiled=True,
    )
    gate_part = jnp.einsum(
        "secd,edf->secf", rows_all, expert_gate, preferred_element_type=jnp.float32
    )
    up_part = jnp.einsum("secd,edf->secf", rows_all, expert_up, preferred_element_type=jnp.float32)
    hidden = silu_gate(gate_part, up_part).astype(jnp.bfloat16)
    hidden_all = gather_directly(hidden, "tp", 3)
    produced = jnp.einsum(
        "secf,efd->secd", hidden_all, expert_down, preferred_element_type=jnp.float32
    ).astype(jnp.bfloat16)
    returned = lax.all_to_all(produced, "sp", split_axis=0, concat_axis=0, tiled=True)
    returned_flat = returned.reshape(experts_all * capacity, local_width)
    picked = returned_flat[targets].astype(jnp.float32).reshape(tok_dev, top_count, local_width)
    routed = jnp.sum(picked * route_weight[:, :, None], axis=1)
    return (mid_wide + shared_out + routed).astype(jnp.bfloat16)


def solution(mesh):
    placed = (
        P("sp", "tp"),
        P("sp", "tp"),
        P("sp", "tp"),
        P("sp", "tp"),
        P("sp", "tp"),
        P(None, "tp"),
        P(),
        P("sp", None),
        P("sp", None),
        P("sp", None, "tp"),
        P("sp", None, "tp"),
        P("sp", None, "tp"),
        P(None, "tp"),
        P(None, "tp"),
        P(None, "tp"),
    )
    return jax.shard_map(
        shards, mesh=mesh, in_specs=placed, out_specs=P("sp", "tp"), check_vma=False
    )
```

profile of v0, /device:TPU:32, one launch (start us, length us, event | category | flops | bytes accessed | tf_op | source)
XLA Modules:
  0.0 489.6 jit_solution(2940403956012515692)
XLA Ops:
  9.9 34.3 %all_gather.13 = f32[16384,1]{0,1:T(1,128)S(1)} all-gather(f32[512,1]{0,1:T(1,128)S(1)} %copy-done.8), channel_id=1, replica_groups=mesh['sp'=32,'tp'=16] {'sp'}, dimensions={0}, use_global_device_ids=true | all-gather | bytes 67584 | tf_op jit(solution)/shard_map/all_gather | solution.py:84
  44.2 43.0 %all-gather.3.cloned.1.call-done = bf16[16384,2,64]{0,2,1:T(8,128)(2,1)} async-done(((bf16[512,2,64]{0,2,1:T(8,128)(2,1)}), bf16[16384,2,64]{0,2,1:T(8,128)(2,1)}) %all-gather.3.cloned.1.call-update) | async-done | bytes 4194320 | tf_op jit(solution)/shard_map/all_gather | solution.py:13
  92.2 49.8 %while.17 = (s32[]{:T(128)}, f32[1,512]{1,0:T(1,128)S(1)}, f32[1,512]{1,0:T(1,128)S(1)}, f32[1,512,64]{1,2,0:T(8,128)S(1)}, s32[32]{0:T(128)S(1)}, /*index=5*/s3...) while((s32[]{:T(128)}, f32[1,512]{1,0:T(1,128)S(1)}, ...), condition=%wide.region_5.6_spmd.clone, body=%wide.region_0.5_spmd.clone.sunk | while | flops 70846464 | bytes 3667313 | solution.py:130
  93.5 2.9 conditional.3
  143.2 6.7 %all-to-all-start = ((bf16[16,512,64]{1,2,0:T(8,128)(2,1)}), bf16[16,512,64]{1,2,0:T(8,128)(2,1)S(1)}, u32[]{:S(2)}, u32[]{:S(2)}) async-start(bf16[16,512,64]{1,2,0:T(8,128)(2,1)} %broadcast_in_dim.50), calls=%async_computation | async-start | bytes 2097152 | tf_op jit(solution)/shard_map/all_to_all | solution.py:28
  150.7 4.3 scatter_custom_fusion
  155.0 11.7 %all-to-all-done = bf16[16,512,64]{1,2,0:T(8,128)(2,1)S(1)} async-done(((bf16[16,512,64]{1,2,0:T(8,128)(2,1)}), bf16[16,512,64]{1,2,0:T(8,128)(2,1)S(1)}, u32[]{:S(2)}, u32[]{:S(2)}) %all-to-all-start) | async-done | bytes 1048608 | tf_op jit(solution)/shard_map/all_to_all | solution.py:28
  167.9 4.5 all-to-all-start.1
  173.2 6.8 %all-to-all-done.1 = f32[16,1,512]{2,1,0:T(1,128)S(1)} async-done(((f32[16,1,512]{2,1,0:T(1,128)}), f32[16,1,512]{2,1,0:T(1,128)S(1)}, u32[]{:S(2)}, u32[]{:S(2)}) %all-to-all-start.1) | async-done | bytes 32800 | tf_op jit(solution)/shard_map/all_to_all | solution.py:28
  183.3 107.7 %all_to_all.31 = bf16[32,4,10,128]{3,1,2,0:T(4,128)(2,1)S(1)} all-to-all(bf16[32,4,10,128]{3,1,2,0:T(4,128)(2,1)S(1)} %copy.81), channel_id=1, replica_groups=mesh['sp'=32,'tp'=16] {'sp'}, dimensions={0} | all-to-all | bytes 655360 | tf_op jit(solution)/shard_map/all_to_all | solution.py:174
  291.8 66.5 %all-gather.5.cloned.1.call-done = bf16[32,4,10,2048]{3,0,2,1:T(8,128)(2,1)} async-done(((bf16[32,4,10,128]{3,0,2,1:T(8,128)(2,1)}), bf16[32,4,10,2048]{3,0,2,1:T(8,128)(2,1)}) %all-gather.5.cloned.1.call-update) | async-done | bytes 5242896 | tf_op jit(solution)/shard_map/all_gather | solution.py:173
  358.3 4.1 convolution_bitcast_fusion.2
  364.0 3.6 broadcast_bitcast_fusion
  367.6 8.3 %reshape.202 = bf16[16,2,20480]{2,1,0:T(2,128)(2,1)} reshape(bf16[16,4,10,32,32]{4,3,2,1,0:T(8,128)(2,1)} %broadcast_bitcast_fusion) | data formatting | bytes 2621440
  375.9 4.9 %all-to-all-start.4 = ((bf16[16,2,20480]{2,1,0:T(2,128)(2,1)}), bf16[16,2,20480]{2,1,0:T(2,128)(2,1)S(1)}, u32[]{:S(2)}, u32[]{:S(2)}) async-start(bf16[16,2,20480]{2,1,0:T(2,128)(2,1)} %reshape.202), calls=%async_computation.4 | async-start | bytes 2621440 | tf_op jit(solution)/shard_map/all_to_all | solution.py:28
  381.0 19.0 %all-to-all-done.4 = bf16[16,2,20480]{2,1,0:T(2,128)(2,1)S(1)} async-done(((bf16[16,2,20480]{2,1,0:T(2,128)(2,1)}), bf16[16,2,20480]{2,1,0:T(2,128)(2,1)S(1)}, u32[]{:S(2)}, u32[]{:S(2)}) %all-to-all-start.4) | async-done | bytes 1310752 | tf_op jit(solution)/shard_map/all_to_all | solution.py:28
  401.7 3.9 all-to-all-start.2
  405.6 7.2 %reshape.203 = bf16[16,4,10,32,32]{4,3,2,1,0:T(8,128)(2,1)} reshape(bf16[16,2,20480]{2,1,0:T(2,128)(2,1)} %copy-done.1) | data formatting | bytes 2621440
  412.9 3.8 bitcast_bitcast_fusion
  416.7 8.4 %copy.83 = bf16[32,4,10,16,32]{4,3,0,2,1:T(8,128)(2,1)} copy(bf16[32,4,10,16,32]{4,0,2,1,3:T(8,128)(2,1)S(1)} %bitcast_bitcast_fusion) | data formatting | bytes 2621440 | tf_op jit(solution)/shard_map/transpose | solution.py:23
  425.0 8.0 %reshape.169 = bf16[32,4,10,512]{3,0,2,1:T(8,128)(2,1)} reshape(bf16[32,4,10,16,32]{4,3,0,2,1:T(8,128)(2,1)} %copy.83) | data formatting | bytes 2621440 | tf_op jit(solution)/shard_map/reshape | solution.py:23
  435.8 12.8 %all-to-all-start.5 = ((bf16[32,4,10,128]{3,1,2,0:T(4,128)(2,1)}), bf16[32,4,10,128]{3,1,2,0:T(4,128)(2,1)S(1)}, u32[]{:S(2)}, u32[]{:S(2)}) async-start(bf16[32,4,10,128]{3,1,2,0:T(4,128)(2,1)} %copy.84), calls=%async_computation.5 | async-start | bytes 655360 | tf_op jit(solution)/shard_map/all_to_all | solution.py:188
  450.7 24.7 %all_gather.14 = bf16[512,512]{0,1:T(8,128)(2,1)S(1)} all-gather(bf16[512,32]{0,1:T(8,128)(2,1)S(1)} %fusion.29), channel_id=1, replica_groups=mesh['sp'=32,'tp'=16] {'tp'}, dimensions={1}, use_global_device_ids=true | all-gather | bytes 557056 | tf_op jit(solution)/shard_map/all_gather | solution.py:154
  475.7 3.2 gather_fusion.1
  (202 shorter events, 61.8 us)
Async XLA Ops:
  6.5 426.5 %copy-start = (bf16[4,512,128]{2,1,0:T(8,128)(2,1)S(1)}, bf16[4,512,128]{2,1,0:T(8,128)(2,1)}, u32[]{:S(2)}) copy-start(bf16[4,512,128]{2,1,0:T(8,128)(2,1)} %param.30) | copy-start | bytes 1572868
  6.5 3.3 copy-start.8
  6.5 80.6 %all-gather.3.cloned.1.call-start = ((), (), s32[]{:S(2)}) async-start(), calls=%async_computation.6 | async-start | bytes 4325376 | tf_op jit(solution)/shard_map/all_gather | solution.py:13
  89.7 2.5 copy-start.12
  142.1 7.9 %copy-start.6 = (s32[512,2]{0,1:T(2,128)S(1)}, s32[512,2]{0,1:T(2,128)}, u32[]{:S(2)}) copy-start(s32[512,2]{0,1:T(2,128)} %param.26) | copy-start | bytes 12292
  142.1 24.6 %copy-start.2 = (bf16[1024,128]{1,0:T(8,128)(2,1)S(1)}, bf16[1024,128]{1,0:T(8,128)(2,1)}, u32[]{:S(2)}) copy-start(bf16[1024,128]{1,0:T(8,128)(2,1)} %param.24) | copy-start | bytes 786436
  142.1 24.6 %copy-start.5 = (bf16[512,128]{1,0:T(8,128)(2,1)S(1)}, bf16[512,128]{1,0:T(8,128)(2,1)}, u32[]{:S(2)}) copy-start(bf16[512,128]{1,0:T(8,128)(2,1)} %param.23) | copy-start | bytes 393220
  143.2 23.5 %all-to-all-start = ((bf16[16,512,64]{1,2,0:T(8,128)(2,1)}), bf16[16,512,64]{1,2,0:T(8,128)(2,1)S(1)}, u32[]{:S(2)}, u32[]{:S(2)}) async-start(bf16[16,512,64]{1,2,0:T(8,128)(2,1)} %broadcast_in_dim.50), calls=%async_computation | async-start | bytes 2097152 | tf_op jit(solution)/shard_map/all_to_all | solution.py:28
  167.9 12.1 %all-to-all-start.1 = ((f32[16,1,512]{2,1,0:T(1,128)}), f32[16,1,512]{2,1,0:T(1,128)S(1)}, u32[]{:S(2)}, u32[]{:S(2)}) async-start(f32[16,1,512]{2,1,0:T(1,128)} %broadcast_in_dim.51), calls=%async_computation.1 | async-start | bytes 65536 | tf_op jit(solution)/shard_map/all_to_all | solution.py:28
  172.4 185.9 %all-gather.5.cloned.1.call-start = ((), (), s32[]{:S(2)}) async-start(), calls=%async_computation.7 | async-start | bytes 5570560 | tf_op jit(solution)/shard_map/all_gather | solution.py:173
  183.0 175.3 %copy-start.10 = (bf16[4,2048,32]{1,2,0:T(8,128)(2,1)S(1)}, bf16[4,2048,32]{1,2,0:T(8,128)(2,1)}, u32[]{:S(2)}) copy-start(bf16[4,2048,32]{1,2,0:T(8,128)(2,1)} %param.28) | copy-start | bytes 1572868
  291.8 70.6 %copy-start.11 = (bf16[4,2048,32]{1,2,0:T(8,128)(2,1)S(1)}, bf16[4,2048,32]{1,2,0:T(8,128)(2,1)}, u32[]{:S(2)}) copy-start(bf16[4,2048,32]{1,2,0:T(8,128)(2,1)} %param.29) | copy-start | bytes 1572868
  358.3 4.2 copy-start.9
  375.9 24.1 %all-to-all-start.4 = ((bf16[16,2,20480]{2,1,0:T(2,128)(2,1)}), bf16[16,2,20480]{2,1,0:T(2,128)(2,1)S(1)}, u32[]{:S(2)}, u32[]{:S(2)}) async-start(bf16[16,2,20480]{2,1,0:T(2,128)(2,1)} %reshape.202), calls=%async_computation.4 | async-start | bytes 2621440 | tf_op jit(solution)/shard_map/all_to_all | solution.py:28
  399.9 1.8 copy-start.1
  401.7 34.1 %all-to-all-start.2 = ((bf16[16,512,128]{1,2,0:T(8,128)(2,1)}), bf16[16,512,128]{1,2,0:T(8,128)(2,1)S(1)}, u32[]{:S(2)}, u32[]{:S(2)}) async-start(bf16[16,512,128]{1,2,0:T(8,128)(2,1)} %broadcast_in_dim.52), calls=%async_computation.2 | async-start | bytes 4194304 | tf_op jit(solution)/shard_map/all_to_all | solution.py:28
  433.0 15.6 %copy-start.7 = (f32[512,2]{0,1:T(2,128)S(1)}, f32[512,2]{0,1:T(2,128)}, u32[]{:S(2)}) copy-start(f32[512,2]{0,1:T(2,128)} %param.27) | copy-start | bytes 12292
  435.8 39.5 %all-to-all-start.5 = ((bf16[32,4,10,128]{3,1,2,0:T(4,128)(2,1)}), bf16[32,4,10,128]{3,1,2,0:T(4,128)(2,1)S(1)}, u32[]{:S(2)}, u32[]{:S(2)}) async-start(bf16[32,4,10,128]{3,1,2,0:T(4,128)(2,1)} %copy.84), calls=%async_computation.5 | async-start | bytes 655360 | tf_op jit(solution)/shard_map/all_to_all | solution.py:188
  448.8 1.4 copy-start.3
  475.5 6.2 %copy-start.4 = (bf16[512,128]{1,0:T(8,128)(2,1)S(1)}, bf16[512,128]{1,0:T(8,128)(2,1)}, u32[]{:S(2)}) copy-start(bf16[512,128]{1,0:T(8,128)(2,1)} %param.33) | copy-start | bytes 393220
Sparse Core Ops, SparseCore 0:
  9.5 77.6 all-gather.2
  291.9 66.3 all-gather.4
where the time goes:
time: 494 us; the launch traced here: 490 us
  blocking collectives  167 us (34%)
  waiting for transfers between devices  147 us (30%)
  local copies, waits for them, and re-layouts  81.5 us (16%)
  starting transfers between devices  32.9 us (7%)
  loops' own time  22.5 us (5%)
  matrix products  18.3 us (4%)
  between operations  13.9 us (3%)
  other arithmetic  6.84 us (1%)
    all_to_all x1, blocking collectives, shards(): lax.all_to_all(outgoing, 'sp', split_axis=0, concat_axis=0, tiled=True)  108 us
    all_gather x1, waiting for transfers between devices, shards(): lax.all_gather(lax.all_to_all(outgoing, 'sp', split_axis=0, concat_axis=0...  66.5 us
    all_gather x1, waiting for transfers between devices, in_one_piece(): filled, at, done = (lax.all_gather(both, axis, axis=dim, tiled=True), 0, [])  43 us
    all_to_all x4, waiting for transfers between devices, sent_to_all(): return lax.all_to_all(copies, axis, split_axis=0, concat_axis=0, tiled=True)  37.5 us
    all_gather x1, blocking collectives, shards(): all_gates = lax.all_gather(log_gate_sums, 'sp', axis=0, tiled=True)  34.3 us
    all_gather x1, blocking collectives, shards(): lax.all_gather(shared_mid, 'tp', axis=1, tiled=True)  24.7 us
    unnamed x32, local copies, waits for them, and re-layouts  22.7 us
    another operation x1, loops' own time, shards(): lax.scan(one_block, initial, (key_blocks, value_blocks, numbers))  22.1 us
  transfers between devices with their start and end apart: 7, of which 5 were waited for; matrix products, arithmetic and copies ran while one was open for 8% of the time, Pallas kernels for 0%

commit v1 on v0

--- a/solution.py
+++ b/solution.py
@@ -150,10 +150,9 @@
         jnp.dot(normed, shared_up, preferred_element_type=jnp.float32),
     ).astype(jnp.bfloat16)
     weight_rows = shared_down
+    sources_all_fit = lambda inp: jnp.concatenate(lax.all_gather(inp, axis_name="tp"), 1)
     shared_out = jnp.dot(
-        lax.all_gather(shared_mid, "tp", axis=1, tiled=True),
-        weight_rows,
-        preferred_element_type=jnp.float32,
+        sources_all_fit(shared_mid), weight_rows, preferred_element_type=jnp.float32
     )
     exp_dev = expert_gate.shape[0]
     sp_count = lax.axis_size("sp")

time: 494 us -> 494 us (level)
  no operation moved by 1% of the time
where the time goes in v1:
time: 494 us; the launch traced here: 490 us
  blocking collectives  167 us (34%)
  waiting for transfers between devices  147 us (30%)
  local copies, waits for them, and re-layouts  81.6 us (17%)
  starting transfers between devices  32.9 us (7%)
  loops' own time  22.5 us (5%)
  matrix products  18.3 us (4%)
  between operations  13.9 us (3%)
  other arithmetic  6.84 us (1%)
    all_to_all x1, blocking collectives, shards(): lax.all_to_all(outgoing, 'sp', split_axis=0, concat_axis=0, tiled=True)  108 us
    all_gather x1, waiting for transfers between devices, shards(): lax.all_gather(lax.all_to_all(outgoing, 'sp', split_axis=0, concat_axis=0...  66.5 us
    all_gather x1, waiting for transfers between devices, in_one_piece(): filled, at, done = (lax.all_gather(both, axis, axis=dim, tiled=True), 0, [])  43 us
    all_to_all x4, waiting for transfers between devices, sent_to_all(): return lax.all_to_all(copies, axis, split_axis=0, concat_axis=0, tiled=True)  37.5 us
    all_gather x1, blocking collectives, shards(): all_gates = lax.all_gather(log_gate_sums, 'sp', axis=0, tiled=True)  34.3 us
    all_gather x1, blocking collectives, shards(): lax.all_gather(inp, axis_name='tp')  24.7 us
    unnamed x32, local copies, waits for them, and re-layouts  22.7 us
    another operation x1, loops' own time, shards(): lax.scan(one_block, initial, (key_blocks, value_blocks, numbers))  22.1 us
  transfers between devices with their start and end apart: 7, of which 5 were waited for; matrix products, arithmetic and copies ran while one was open for 8% of the time, Pallas kernels for 0%

profile of v1, /device:TPU:32, one launch (start us, length us, event | category | flops | bytes accessed | tf_op | source)
XLA Modules:
  0.0 489.6 jit_solution(2269844680615917342)
XLA Ops:
  9.9 34.3 %all_gather.16 = f32[16384,1]{0,1:T(1,128)S(1)} all-gather(f32[512,1]{0,1:T(1,128)S(1)} %copy-done.8), channel_id=1, replica_groups=mesh['sp'=32,'tp'=16] {'sp'}, dimensions={0}, use_global_device_ids=true | all-gather | bytes 67584 | tf_op jit(solution)/shard_map/all_gather | solution.py:84
  44.2 43.0 %all-gather.4.cloned.1.call-done = bf16[16384,2,64]{0,2,1:T(8,128)(2,1)} async-done(((bf16[512,2,64]{0,2,1:T(8,128)(2,1)}), bf16[16384,2,64]{0,2,1:T(8,128)(2,1)}) %all-gather.4.cloned.1.call-update) | async-done | bytes 4194320 | tf_op jit(solution)/shard_map/all_gather | solution.py:13
  92.2 49.8 %while.17 = (s32[]{:T(128)}, f32[1,512]{1,0:T(1,128)S(1)}, f32[1,512]{1,0:T(1,128)S(1)}, f32[1,512,64]{1,2,0:T(8,128)S(1)}, s32[32]{0:T(128)S(1)}, /*index=5*/s3...) while((s32[]{:T(128)}, f32[1,512]{1,0:T(1,128)S(1)}, ...), condition=%wide.region_5.6_spmd.clone, body=%wide.region_0.5_spmd.clone.sunk | while | flops 70846464 | bytes 3667313 | solution.py:130
  93.5 2.9 conditional.3
  143.2 6.7 %all-to-all-start = ((bf16[16,512,64]{1,2,0:T(8,128)(2,1)}), bf16[16,512,64]{1,2,0:T(8,128)(2,1)S(1)}, u32[]{:S(2)}, u32[]{:S(2)}) async-start(bf16[16,512,64]{1,2,0:T(8,128)(2,1)} %broadcast_in_dim.50), calls=%async_computation | async-start | bytes 2097152 | tf_op jit(solution)/shard_map/all_to_all | solution.py:28
  150.7 4.3 scatter_custom_fusion
  155.0 11.7 %all-to-all-done = bf16[16,512,64]{1,2,0:T(8,128)(2,1)S(1)} async-done(((bf16[16,512,64]{1,2,0:T(8,128)(2,1)}), bf16[16,512,64]{1,2,0:T(8,128)(2,1)S(1)}, u32[]{:S(2)}, u32[]{:S(2)}) %all-to-all-start) | async-done | bytes 1048608 | tf_op jit(solution)/shard_map/all_to_all | solution.py:28
  167.9 4.5 all-to-all-start.1
  173.2 6.8 %all-to-all-done.1 = f32[16,1,512]{2,1,0:T(1,128)S(1)} async-done(((f32[16,1,512]{2,1,0:T(1,128)}), f32[16,1,512]{2,1,0:T(1,128)S(1)}, u32[]{:S(2)}, u32[]{:S(2)}) %all-to-all-start.1) | async-done | bytes 32800 | tf_op jit(solution)/shard_map/all_to_all | solution.py:28
  183.3 107.7 %all_to_all.31 = bf16[32,4,10,128]{3,1,2,0:T(4,128)(2,1)S(1)} all-to-all(bf16[32,4,10,128]{3,1,2,0:T(4,128)(2,1)S(1)} %copy.86), channel_id=1, replica_groups=mesh['sp'=32,'tp'=16] {'sp'}, dimensions={0} | all-to-all | bytes 655360 | tf_op jit(solution)/shard_map/all_to_all | solution.py:173
  291.8 66.5 %all-gather.6.cloned.1.call-done = bf16[32,4,10,2048]{3,0,2,1:T(8,128)(2,1)} async-done(((bf16[32,4,10,128]{3,0,2,1:T(8,128)(2,1)}), bf16[32,4,10,2048]{3,0,2,1:T(8,128)(2,1)}) %all-gather.6.cloned.1.call-update) | async-done | bytes 5242896 | tf_op jit(solution)/shard_map/all_gather | solution.py:172
  358.3 4.1 convolution_bitcast_fusion.2
  364.0 3.6 broadcast_bitcast_fusion
  367.6 8.3 %reshape.211 = bf16[16,2,20480]{2,1,0:T(2,128)(2,1)} reshape(bf16[16,4,10,32,32]{4,3,2,1,0:T(8,128)(2,1)} %broadcast_bitcast_fusion) | data formatting | bytes 2621440
  375.9 4.9 %all-to-all-start.4 = ((bf16[16,2,20480]{2,1,0:T(2,128)(2,1)}), bf16[16,2,20480]{2,1,0:T(2,128)(2,1)S(1)}, u32[]{:S(2)}, u32[]{:S(2)}) async-start(bf16[16,2,20480]{2,1,0:T(2,128)(2,1)} %reshape.211), calls=%async_computation.4 | async-start | bytes 2621440 | tf_op jit(solution)/shard_map/all_to_all | solution.py:28
  381.0 19.0 %all-to-all-done.4 = bf16[16,2,20480]{2,1,0:T(2,128)(2,1)S(1)} async-done(((bf16[16,2,20480]{2,1,0:T(2,128)(2,1)}), bf16[16,2,20480]{2,1,0:T(2,128)(2,1)S(1)}, u32[]{:S(2)}, u32[]{:S(2)}) %all-to-all-start.4) | async-done | bytes 1310752 | tf_op jit(solution)/shard_map/all_to_all | solution.py:28
  401.7 3.9 all-to-all-start.2
  405.6 7.2 %reshape.212 = bf16[16,4,10,32,32]{4,3,2,1,0:T(8,128)(2,1)} reshape(bf16[16,2,20480]{2,1,0:T(2,128)(2,1)} %copy-done.1) | data formatting | bytes 2621440
  412.9 3.8 bitcast_bitcast_fusion
  416.7 8.4 %copy.88 = bf16[32,4,10,16,32]{4,3,0,2,1:T(8,128)(2,1)} copy(bf16[32,4,10,16,32]{4,0,2,1,3:T(8,128)(2,1)S(1)} %bitcast_bitcast_fusion) | data formatting | bytes 2621440 | tf_op jit(solution)/shard_map/transpose | solution.py:23
  425.0 8.0 %reshape.177 = bf16[32,4,10,512]{3,0,2,1:T(8,128)(2,1)} reshape(bf16[32,4,10,16,32]{4,3,0,2,1:T(8,128)(2,1)} %copy.88) | data formatting | bytes 2621440 | tf_op jit(solution)/shard_map/reshape | solution.py:23
  435.8 12.8 %all-to-all-start.5 = ((bf16[32,4,10,128]{3,1,2,0:T(4,128)(2,1)}), bf16[32,4,10,128]{3,1,2,0:T(4,128)(2,1)S(1)}, u32[]{:S(2)}, u32[]{:S(2)}) async-start(bf16[32,4,10,128]{3,1,2,0:T(4,128)(2,1)} %copy.89), calls=%async_computation.5 | async-start | bytes 655360 | tf_op jit(solution)/shard_map/all_to_all | solution.py:187
  450.7 24.7 %all-gather = bf16[8192,32]{0,1:T(8,128)(2,1)S(1)} all-gather(bf16[512,32]{0,1:T(8,128)(2,1)S(1)} %fusion.29), channel_id=2, replica_groups=mesh['sp'=32,'tp'=16] {'tp'}, dimensions={0}, use_global_device_ids=true | all-gather | bytes 557056 | tf_op jit(solution)/shard_map/all_gather | solution.py:153
  475.7 3.2 gather_fusion.1
  (203 shorter events, 61.9 us)
Async XLA Ops:
  6.5 426.5 %copy-start = (bf16[4,512,128]{2,1,0:T(8,128)(2,1)S(1)}, bf16[4,512,128]{2,1,0:T(8,128)(2,1)}, u32[]{:S(2)}) copy-start(bf16[4,512,128]{2,1,0:T(8,128)(2,1)} %param.30) | copy-start | bytes 1572868
  6.5 3.3 copy-start.8
  6.5 80.6 %all-gather.4.cloned.1.call-start = ((), (), s32[]{:S(2)}) async-start(), calls=%async_computation.6 | async-start | bytes 4325376 | tf_op jit(solution)/shard_map/all_gather | solution.py:13
  89.7 2.5 copy-start.12
  142.1 7.9 %copy-start.6 = (s32[512,2]{0,1:T(2,128)S(1)}, s32[512,2]{0,1:T(2,128)}, u32[]{:S(2)}) copy-start(s32[512,2]{0,1:T(2,128)} %param.26) | copy-start | bytes 12292
  142.1 24.6 %copy-start.2 = (bf16[1024,128]{1,0:T(8,128)(2,1)S(1)}, bf16[1024,128]{1,0:T(8,128)(2,1)}, u32[]{:S(2)}) copy-start(bf16[1024,128]{1,0:T(8,128)(2,1)} %param.24) | copy-start | bytes 786436
  142.1 24.6 %copy-start.5 = (bf16[512,128]{1,0:T(8,128)(2,1)S(1)}, bf16[512,128]{1,0:T(8,128)(2,1)}, u32[]{:S(2)}) copy-start(bf16[512,128]{1,0:T(8,128)(2,1)} %param.23) | copy-start | bytes 393220
  143.2 23.5 %all-to-all-start = ((bf16[16,512,64]{1,2,0:T(8,128)(2,1)}), bf16[16,512,64]{1,2,0:T(8,128)(2,1)S(1)}, u32[]{:S(2)}, u32[]{:S(2)}) async-start(bf16[16,512,64]{1,2,0:T(8,128)(2,1)} %broadcast_in_dim.50), calls=%async_computation | async-start | bytes 2097152 | tf_op jit(solution)/shard_map/all_to_all | solution.py:28
  167.9 12.1 %all-to-all-start.1 = ((f32[16,1,512]{2,1,0:T(1,128)}), f32[16,1,512]{2,1,0:T(1,128)S(1)}, u32[]{:S(2)}, u32[]{:S(2)}) async-start(f32[16,1,512]{2,1,0:T(1,128)} %broadcast_in_dim.51), calls=%async_computation.1 | async-start | bytes 65536 | tf_op jit(solution)/shard_map/all_to_all | solution.py:28
  172.4 185.9 %all-gather.6.cloned.1.call-start = ((), (), s32[]{:S(2)}) async-start(), calls=%async_computation.7 | async-start | bytes 5570560 | tf_op jit(solution)/shard_map/all_gather | solution.py:172
  183.0 175.3 %copy-start.10 = (bf16[4,2048,32]{1,2,0:T(8,128)(2,1)S(1)}, bf16[4,2048,32]{1,2,0:T(8,128)(2,1)}, u32[]{:S(2)}) copy-start(bf16[4,2048,32]{1,2,0:T(8,128)(2,1)} %param.28) | copy-start | bytes 1572868
  291.8 70.6 %copy-start.11 = (bf16[4,2048,32]{1,2,0:T(8,128)(2,1)S(1)}, bf16[4,2048,32]{1,2,0:T(8,128)(2,1)}, u32[]{:S(2)}) copy-start(bf16[4,2048,32]{1,2,0:T(8,128)(2,1)} %param.29) | copy-start | bytes 1572868
  358.3 4.2 copy-start.9
  375.9 24.1 %all-to-all-start.4 = ((bf16[16,2,20480]{2,1,0:T(2,128)(2,1)}), bf16[16,2,20480]{2,1,0:T(2,128)(2,1)S(1)}, u32[]{:S(2)}, u32[]{:S(2)}) async-start(bf16[16,2,20480]{2,1,0:T(2,128)(2,1)} %reshape.211), calls=%async_computation.4 | async-start | bytes 2621440 | tf_op jit(solution)/shard_map/all_to_all | solution.py:28
  399.9 1.8 copy-start.1
  401.7 34.1 %all-to-all-start.2 = ((bf16[16,512,128]{1,2,0:T(8,128)(2,1)}), bf16[16,512,128]{1,2,0:T(8,128)(2,1)S(1)}, u32[]{:S(2)}, u32[]{:S(2)}) async-start(bf16[16,512,128]{1,2,0:T(8,128)(2,1)} %broadcast_in_dim.52), calls=%async_computation.2 | async-start | bytes 4194304 | tf_op jit(solution)/shard_map/all_to_all | solution.py:28
  433.0 15.6 %copy-start.7 = (f32[512,2]{0,1:T(2,128)S(1)}, f32[512,2]{0,1:T(2,128)}, u32[]{:S(2)}) copy-start(f32[512,2]{0,1:T(2,128)} %param.27) | copy-start | bytes 12292
  435.8 39.6 %all-to-all-start.5 = ((bf16[32,4,10,128]{3,1,2,0:T(4,128)(2,1)}), bf16[32,4,10,128]{3,1,2,0:T(4,128)(2,1)S(1)}, u32[]{:S(2)}, u32[]{:S(2)}) async-start(bf16[32,4,10,128]{3,1,2,0:T(4,128)(2,1)} %copy.89), calls=%async_computation.5 | async-start | bytes 655360 | tf_op jit(solution)/shard_map/all_to_all | solution.py:187
  448.8 1.4 copy-start.3
  475.6 6.2 %copy-start.4 = (bf16[512,128]{1,0:T(8,128)(2,1)S(1)}, bf16[512,128]{1,0:T(8,128)(2,1)}, u32[]{:S(2)}) copy-start(bf16[512,128]{1,0:T(8,128)(2,1)} %param.33) | copy-start | bytes 393220
Sparse Core Ops, SparseCore 0:
  9.5 77.6 all-gather.3
  291.9 66.3 all-gather.5
